TPU v7x, 32 devices: a whole 2x2x4 slice. The times are simulated.
32 devices in a mesh: rep: 2 (over x), fs: 8 (over z, y), tp: 2 (over core).
Axes of the slice: x: 2, y: 2, z: 4, core: 2. Of those that a mesh axis runs over, the one named last changes fastest.
Arguments:
- tokens: bfloat16 [16384, 2048], P(('rep', 'fs')), may hold values from -6 to 6
- norm_mix: bfloat16 [2048], replicated, may hold values from 0.099609375 to 1.8984375
- w_unit: bfloat16 [2048, 1024], P('fs', 'tp'), may hold values from -0.125 to 0.125
- w_value: bfloat16 [2048, 1024], P('fs', 'tp'), may hold values from -0.125 to 0.125
- spatial: bfloat16 [4, 128, 128], replicated, may hold values from -0.52734375 to 0.52734375
- spatial_bias: bfloat16 [4, 128], replicated, may hold values from 0.099609375 to 1.8984375
- group_gain: bfloat16 [1024], replicated, may hold values from 0.099609375 to 1.8984375
- group_shift: bfloat16 [1024], replicated, may hold values from -3 to 3
- w_mix_out: bfloat16 [1024, 2048], P('tp', 'fs'), may hold values from -0.1875 to 0.1875
- norm_ffn: bfloat16 [2048], replicated, may hold values from 0.099609375 to 1.8984375
- w_gate: bfloat16 [2048, 2816], P('fs', 'tp'), may hold values from -0.125 to 0.125
- w_up: bfloat16 [2048, 2816], P('fs', 'tp'), may hold values from -0.125 to 0.125
- w_down: bfloat16 [2816, 2048], P('tp', 'fs'), may hold values from -0.109375 to 0.109375
Outputs:
- layer_out: bfloat16 [16384, 2048], P(('rep', 'fs', 'tp'))
All inputs are finite; a program needn't handle non-finite values.
Results may differ from a plain program's by a relative error of at most 0.008.
Values may be sent and summed in bfloat16 or wider, within the bound.
A program may use at most 128 MiB of HBM per device.

v0:
```python
import jax
import jax.numpy as jnp
from jax import lax
from jax.sharding import PartitionSpec as P


def rms_scale(values, gain):
    values = values.astype(jnp.float32)
    scale = lax.rsqrt(jnp.mean(values * values, axis=-1, keepdims=True) + 1e-06)
    return values * scale * gain.astype(jnp.float32)


def spatial_unit(unit_pre, value_pre, spatial, spatial_bias, group_gain, group_shift):
    count, width = value_pre.shape
    groups = spatial.shape[0]
    block = spatial.shape[1]
    active = jax.nn.gelu(value_pre, approximate=True).reshape(count, groups, width // groups)
    center = jnp.mean(active, axis=-1, keepdims=True)
    spread = jnp.mean(jnp.square(active - center), axis=-1, keepdims=True)
    normal = ((active - center) * lax.rsqrt(spread + 1e-06)).reshape(count, width)
    normal = normal * group_gain.astype(jnp.float32) + group_shift.astype(jnp.float32)
    grouped = normal.astype(jnp.bfloat16)
    causal = jnp.tril(jnp.ones((block, block), dtype=bool))
    weights = jnp.where(causal[None], spatial, jnp.zeros_like(spatial))
    tiles = grouped.reshape(count // block, block, groups, width // groups)
    mixed = jnp.einsum("gts,nsgd->ntgd", weights, tiles, preferred_element_type=jnp.float32)
    mixed = mixed + spatial_bias.astype(jnp.float32).T[None, :, :, None]
    return jax.nn.gelu(unit_pre, approximate=True) * mixed.reshape(count, width)


def on_device(
    tokens,
    norm_mix,
    w_unit,
    w_value,
    spatial,
    spatial_bias,
    group_gain,
    group_shift,
    w_mix_out,
    norm_ffn,
    w_gate,
    w_up,
    w_down,
):
    count = tokens.shape[0]
    half = count // lax.axis_size("tp")
    position = lax.axis_index("tp")
    row_start = position * half
    local_width = w_unit.shape[1]
    group_count = spatial.shape[0] // lax.axis_size("tp")
    group_start = position * group_count
    spatial_local = lax.dynamic_slice_in_dim(spatial, group_start, group_count, 0)
    bias_local = lax.dynamic_slice_in_dim(spatial_bias, group_start, group_count, 0)
    gain_local = lax.dynamic_slice_in_dim(group_gain, position * local_width, local_width, 0)
    shift_local = lax.dynamic_slice_in_dim(group_shift, position * local_width, local_width, 0)
    normed = rms_scale(tokens, norm_mix).astype(jnp.bfloat16)
    unit_whole, value_whole = (
        lax.all_gather(w_unit, "fs", axis=0, tiled=True),
        lax.all_gather(w_value, "fs", axis=0, tiled=True),
    )
    unit_pre = jnp.dot(normed, unit_whole, preferred_element_type=jnp.float32)
    value_pre = jnp.dot(normed, value_whole, preferred_element_type=jnp.float32)
    gated = spatial_unit(
        unit_pre, value_pre, spatial_local, bias_local, gain_local, shift_local
    ).astype(jnp.bfloat16)
    token_rows = lax.all_to_all(gated, "tp", split_axis=0, concat_axis=1, tiled=True)
    out_columns = lax.all_gather(w_mix_out, "fs", axis=1, tiled=True)
    out_whole = lax.all_gather(out_columns, "tp", axis=0, tiled=True)
    own_rows = lax.dynamic_slice_in_dim(tokens, row_start, half, 0)
    own_mid = (
        own_rows.astype(jnp.float32)
        + jnp.dot(token_rows, out_whole, preferred_element_type=jnp.float32)
    ).astype(jnp.bfloat16)
    h_mid = lax.all_gather(own_mid, "tp", axis=0, tiled=True)
    normed_mid = rms_scale(h_mid, norm_ffn).astype(jnp.bfloat16)
    gate_whole, up_whole = (
        lax.all_gather(w_gate, "fs", axis=0, tiled=True),
        lax.all_gather(w_up, "fs", axis=0, tiled=True),
    )
    gate = jnp.dot(normed_mid, gate_whole, preferred_element_type=jnp.float32)
    up = jnp.dot(normed_mid, up_whole, preferred_element_type=jnp.float32)
    hidden = (jax.nn.silu(gate) * up).astype(jnp.bfloat16)
    down_cols = lax.all_gather(w_down, "fs", axis=1, tiled=True)
    residual_rows = lax.dynamic_slice_in_dim(h_mid, row_start, half, 0).astype(jnp.float32)
    hidden_rows = lax.all_to_all(hidden, "tp", split_axis=0, concat_axis=1, tiled=True)
    down_full = lax.all_gather(down_cols, "tp", axis=0, tiled=True)
    summed_rows = jnp.dot(hidden_rows, down_full, preferred_element_type=jnp.float32)
    return (residual_rows + summed_rows).astype(jnp.bfloat16)


def solution(mesh):
    placed = (
        P(("rep", "fs"), None),
        P(),
        P("fs", "tp"),
        P("fs", "tp"),
        P(),
        P(),
        P(),
        P(),
        P("tp", "fs"),
        P(),
        P("fs", "tp"),
        P("fs", "tp"),
        P("tp", "fs"),
    )
    return jax.shard_map(
        on_device,
        mesh=mesh,
        in_specs=placed,
        out_specs=P(("rep", "fs", "tp"), None),
        check_vma=False,
    )
```

profile of v0, /device:TPU:0, one launch (start us, length us, event | category | flops | bytes accessed | tf_op | source)
XLA Modules:
  0.0 516.4 jit_solution(7229913326769791295)
XLA Ops:
  6.5 0.0 all-gather.14.cloned.1.call-start
  6.5 0.7 all-gather.14.cloned.1.call-update
  7.3 0.0 all-gather.12.cloned.1.call-start
  7.3 0.7 all-gather.12.cloned.1.call-update
  8.0 0.0 all-gather.10.cloned.1.call-start
  8.1 0.7 all-gather.10.cloned.1.call-update
  8.7 0.0 all-gather.16.cloned.1.call-start
  8.8 53.7 %all-gather.14.cloned.1.call-done = bf16[512,2048]{1,0:T(8,128)(2,1)} async-done(((bf16[512,256]{1,0:T(8,128)(2,1)}), bf16[512,2048]{1,0:T(8,128)(2,1)}) %all-gather.14.cloned.1.call-update) | async-done | bytes 2097168 | tf_op jit(solution)/shard_map/all_gather | solution.py:68
  62.5 0.0 all-gather.16.cloned.1.call-update
  62.5 0.0 all-gather.24.cloned.1.call-start
  62.5 0.5 all-gather.24.cloned.1.call-update
  63.1 0.0 all-gather.18.cloned.1.call-start
  63.1 0.7 convert_element_type.48
  63.8 0.7 convert_bitcast_fusion
  64.5 0.8 dynamic-slice_convert_fusion
  65.3 3.1 fusion
  68.4 43.5 %all-gather.12.cloned.1.call-done = bf16[2048,512]{1,0:T(8,128)(2,1)} async-done(((bf16[256,512]{1,0:T(8,128)(2,1)}), bf16[2048,512]{1,0:T(8,128)(2,1)}) %all-gather.12.cloned.1.call-update) | async-done | bytes 2097168 | tf_op jit(solution)/shard_map/all_gather | solution.py:60
  111.9 6.9 %fusion.21 = f32[1024,512]{1,0:T(8,128)} fusion(bf16[2048,512]{1,0:T(8,128)(2,1)} %all-gather.12.cloned.1.call-done, bf16[1024,2048]{1,0:T(8,128)(2,1)} %param.13, f32[2048]{0:T(1024)S(1)} %convert_element_type.48, f32[1024]{0:T(1024)S(1)} %add_rsqrt_fusion.2), kind=kOutput, calls=%fused_computation.30 | convolution fusion | flops 2160066560 | bytes 8400896 | tf_op jit(solution)/shard_map/dot_general | solution.py:63
  118.8 2.6 reshape.58
  121.4 1.2 reduce_sum.37
  122.6 14.4 %multiply_reduce_fusion = f32[1024,2]{1,0:T(8,128)S(1)} fusion(f32[1024,2,256]{2,1,0:T(2,128)S(1)} %reshape.58, f32[1024,2]{1,0:T(8,128)S(1)} %broadcast_multiply_fusion), kind=kLoop, calls=%fused_computation.33 | loop fusion | flops 1570816 | bytes 2113536 | tf_op jit(solution)/shard_map/reduce_sum | solution.py:19
  137.1 0.1 add_rsqrt_fusion
  137.2 1.2 mul.113
  138.4 0.2 copy.33
  138.6 0.0 copy-start
  138.6 1.2 sub.17
  139.9 0.2 copy.32
  140.0 0.4 copy-done
  140.4 0.0 copy-start.1
  140.4 0.8 add_convert_fusion.2
  141.3 0.3 reshape.59
  141.6 0.0 copy-done.1
  141.6 0.5 bitcast_add_fusion
  142.1 2.3 copy.27
  144.4 1.8 copy.34
  146.2 15.5 %all-gather.10.cloned.1.call-done = bf16[2048,512]{1,0:T(8,128)(2,1)} async-done(((bf16[256,512]{1,0:T(8,128)(2,1)}), bf16[2048,512]{1,0:T(8,128)(2,1)}) %all-gather.10.cloned.1.call-update) | async-done | bytes 2097168 | tf_op jit(solution)/shard_map/all_gather | solution.py:59
  161.7 5.7 %fusion.14 = bf16[1024,512]{1,0:T(8,128)(2,1)S(1)} fusion(f32[1024,512]{1,0:T(8,128)S(1)} %bitcast.40, bf16[2048,512]{1,0:T(8,128)(2,1)} %all-gather.10.cloned.1.call-done, bf16[1024,2048]{1,0:T(8,128)(2,1)} %param.13, f32[2048]{0:T(1024)S(1)} %convert_element_type.48, f32[1024]{0:T(1024)S(1)} %add_rsqrt_fusion.2), kind=kOutput, calls=%fused_computation.23 | convolution fusion | flops 2161115136 | bytes 9449472 | tf_op jit(solution)/shard_map/dot_general | solution.py:62
  167.4 0.5 copy.28
  168.0 4.6 all_to_all.38
  172.5 2.8 all-gather.16.cloned.1.call-done
  175.3 6.6 %add_convert_fusion.1 = bf16[512,2048]{1,0:T(8,128)(2,1)} fusion(bf16[512,1024]{0,1:T(8,128)(2,1)S(1)} %bitcast.37, bf16[1024,2048]{1,0:T(8,128)(2,1)} %all-gather.16.cloned.1.call-done, bf16[1024,2048]{1,0:T(8,128)(2,1)} %param.13, s32[]{:T(128)S(6)} %select_n.16), kind=kOutput, calls=%fused_computation.12 | convolution fusion | flops 2150629376 | bytes 9437188 | tf_op jit(solution)/shard_map/dot_general | solution.py:73
  181.9 0.0 copy-start.2
  181.9 0.0 all-gather.18.cloned.1.call-update
  181.9 0.0 all-gather.20.cloned.1.call-start
  182.0 0.7 all-gather.20.cloned.1.call-update
  182.7 0.0 all-gather.22.cloned.1.call-start
  182.7 0.7 all-gather.22.cloned.1.call-update
  183.4 0.0 all-gather.26.cloned.1.call-start
  183.5 88.1 %all-gather.24.cloned.1.call-done = bf16[1408,2048]{1,0:T(8,128)(2,1)} async-done(((bf16[1408,256]{1,0:T(8,128)(2,1)}), bf16[1408,2048]{1,0:T(8,128)(2,1)}) %all-gather.24.cloned.1.call-update) | async-done | bytes 5767184 | tf_op jit(solution)/shard_map/all_gather | solution.py:84
  271.6 0.0 all-gather.26.cloned.1.call-update
  271.6 0.0 copy-done.2
  271.6 13.2 %all-gather.18.cloned.1.call-done = bf16[1024,2048]{1,0:T(8,128)(2,1)} async-done(((bf16[512,2048]{1,0:T(8,128)(2,1)}), bf16[1024,2048]{1,0:T(8,128)(2,1)}) %all-gather.18.cloned.1.call-update) | async-done | bytes 4194320 | tf_op jit(solution)/shard_map/all_gather | solution.py:75
  284.8 3.1 fusion.3
  287.9 92.6 %all-gather.20.cloned.1.call-done = bf16[2048,1408]{1,0:T(8,128)(2,1)} async-done(((bf16[256,1408]{1,0:T(8,128)(2,1)}), bf16[2048,1408]{1,0:T(8,128)(2,1)}) %all-gather.20.cloned.1.call-update) | async-done | bytes 5767184 | tf_op jit(solution)/shard_map/all_gather | solution.py:78
  380.5 11.9 %fusion.23 = f32[1024,1408]{1,0:T(8,128)} fusion(bf16[2048,1408]{1,0:T(8,128)(2,1)} %all-gather.20.cloned.1.call-done, bf16[1024,2048]{1,0:T(8,128)(2,1)} %all-gather.18.cloned.1.call-done, f32[2048]{0:T(1024)S(1)} %convert_element_type.57, f32[1024]{0:T(1024)S(1)} %add_rsqrt_fusion.1), kind=kOutput, calls=%fused_computation.34 | convolution fusion | flops 5913968640 | bytes 15740928 | tf_op jit(solution)/shard_map/dot_general | solution.py:81
  392.4 80.8 %all-gather.22.cloned.1.call-done = bf16[2048,1408]{1,0:T(8,128)(2,1)} async-done(((bf16[256,1408]{1,0:T(8,128)(2,1)}), bf16[2048,1408]{1,0:T(8,128)(2,1)}) %all-gather.22.cloned.1.call-update) | async-done | bytes 5767184 | tf_op jit(solution)/shard_map/all_gather | solution.py:79
  473.2 12.5 %multiply_convert_fusion = bf16[1024,1408]{1,0:T(8,128)(2,1)} fusion(f32[1024,1408]{1,0:T(8,128)} %fusion.23, bf16[2048,1408]{1,0:T(8,128)(2,1)} %all-gather.22.cloned.1.call-done, bf16[1024,2048]{1,0:T(8,128)(2,1)} %all-gather.18.cloned.1.call-done, f32[2048]{0:T(1024)S(1)} %convert_element_type.57, f32[1024]{0:T(1024)S(1)} %add_rsqrt_fusion.1), kind=kOutput, calls=%fused_computation.10 | convolution fusion | flops 5922619392 | bytes 18624512 | tf_op jit(solution)/shard_map/dot_general | solution.py:82
  485.7 3.4 copy.29
  489.2 9.1 %all_to_all.39 = bf16[2,512,1408]{1,2,0:T(8,128)(2,1)} all-to-all(bf16[2,512,1408]{1,2,0:T(8,128)(2,1)S(1)} %copy.29), channel_id=1, replica_groups=mesh['rep'=2,'fs'=8,'tp'=2] {'tp'}, dimensions={0} | all-to-all | bytes 5767168 | tf_op jit(solution)/shard_map/all_to_all | solution.py:86
  498.3 0.5 all-gather.26.cloned.1.call-done
  498.8 11.1 %add_convert_fusion = bf16[512,2048]{1,0:T(8,128)(2,1)} fusion(bf16[512,2816]{0,1:T(8,128)(2,1)} %bitcast.38, bf16[2816,2048]{1,0:T(8,128)(2,1)} %all-gather.26.cloned.1.call-done, bf16[1024,2048]{1,0:T(8,128)(2,1)} %all-gather.18.cloned.1.call-done, s32[]{:T(128)S(6)} %select_n.16), kind=kOutput, calls=%fused_computation.11 | convolution fusion | flops 5908725760 | bytes 18612228 | tf_op jit(solution)/shard_map/dot_general | solution.py:88
  (5 shorter events, 0.1 us)
Async XLA Ops:
  6.5 55.9 %all-gather.14.cloned.1.call-start = ((), (), s32[]{:S(2)}) async-start(), calls=%async_computation.4 | async-start | bytes 2359296 | tf_op jit(solution)/shard_map/all_gather | solution.py:68
  7.3 104.7 %all-gather.12.cloned.1.call-start = ((), (), s32[]{:S(2)}) async-start(), calls=%async_computation.3 | async-start | bytes 2359296 | tf_op jit(solution)/shard_map/all_gather | solution.py:60
  8.0 153.7 %all-gather.10.cloned.1.call-start = ((), (), s32[]{:S(2)}) async-start(), calls=%async_computation.2 | async-start | bytes 2359296 | tf_op jit(solution)/shard_map/all_gather | solution.py:59
  8.7 166.6 %all-gather.16.cloned.1.call-start = ((), (), s32[]{:S(2)}) async-start(), calls=%async_computation.5 | async-start | bytes 6291456 | tf_op jit(solution)/shard_map/all_gather | solution.py:69
  62.5 209.1 %all-gather.24.cloned.1.call-start = ((), (), s32[]{:S(2)}) async-start(), calls=%async_computation.9 | async-start | bytes 6488064 | tf_op jit(solution)/shard_map/all_gather | solution.py:84
  63.1 221.8 %all-gather.18.cloned.1.call-start = ((), (), s32[]{:S(2)}) async-start(), calls=%async_computation.6 | async-start | bytes 6291456 | tf_op jit(solution)/shard_map/all_gather | solution.py:75
  138.6 1.8 copy-start
  140.4 1.1 copy-start.1
  181.9 89.7 %copy-start.2 = (bf16[2048]{0:T(1024)(128)(2,1)S(1)}, bf16[2048]{0:T(1024)(128)(2,1)}, u32[]{:S(2)}) copy-start(bf16[2048]{0:T(1024)(128)(2,1)} %param.22) | copy-start | bytes 12292
  181.9 198.6 %all-gather.20.cloned.1.call-start = ((), (), s32[]{:S(2)}) async-start(), calls=%async_computation.7 | async-start | bytes 6488064 | tf_op jit(solution)/shard_map/all_gather | solution.py:78
  182.7 290.6 %all-gather.22.cloned.1.call-start = ((), (), s32[]{:S(2)}) async-start(), calls=%async_computation.8 | async-start | bytes 6488064 | tf_op jit(solution)/shard_map/all_gather | solution.py:79
  183.4 315.3 %all-gather.26.cloned.1.call-start = ((), (), s32[]{:S(2)}) async-start(), calls=%async_computation.10 | async-start | bytes 17301504 | tf_op jit(solution)/shard_map/all_gather | solution.py:87
Sparse Core Ops, SparseCore 0:
  9.4 53.0 all-gather.13
  64.6 47.2 all-gather.11
  114.0 47.6 all-gather.9
  163.1 12.1 all-gather.15
  177.2 94.2 all-gather.23
  273.0 11.8 all-gather.17
  287.0 93.4 all-gather.19
  382.7 90.4 all-gather.21
  474.8 23.8 all-gather.25
where the time goes:
time: 517 us; the launch traced here: 516 us
  waiting for transfers between devices  395 us (76%)
  matrix products  55.2 us (11%)
  other arithmetic  24.9 us (5%)
  local copies, waits for them, and re-layouts  14.2 us (3%)
  blocking collectives  13.7 us (3%)
  between operations  13.4 us (3%)
    all_gather x1, waiting for transfers between devices, on_device(): lax.all_gather(w_gate, 'fs', axis=0, tiled=True)  92.6 us
    all_gather x1, waiting for transfers between devices, on_device(): down_cols = lax.all_gather(w_down, 'fs', axis=1, tiled=True)  88.1 us
    all_gather x1, waiting for transfers between devices, on_device(): lax.all_gather(w_up, 'fs', axis=0, tiled=True)  80.8 us
    all_gather x1, waiting for transfers between devices, on_device(): out_columns = lax.all_gather(w_mix_out, 'fs', axis=1, tiled=True)  53.7 us
    all_gather x1, waiting for transfers between devices, on_device(): lax.all_gather(w_value, 'fs', axis=0, tiled=True)  43.5 us
    all_gather x1, waiting for transfers between devices, on_device(): lax.all_gather(w_unit, 'fs', axis=0, tiled=True)  15.5 us
    reduce_sum x1, other arithmetic, spatial_unit(): spread = jnp.mean(jnp.square(active - center), axis=-1, keepdims=True)  14.4 us
    all_gather x1, waiting for transfers between devices, on_device(): h_mid = lax.all_gather(own_mid, 'tp', axis=0, tiled=True)  13.2 us
  transfers between devices with their start and end apart: 9, of which 9 were waited for; matrix products, arithmetic and copies ran while one was open for 16% of the time, Pallas kernels for 0%

commit v1 on v0

--- a/solution.py
+++ b/solution.py
@@ -65,7 +65,8 @@
         unit_pre, value_pre, spatial_local, bias_local, gain_local, shift_local
     ).astype(jnp.bfloat16)
     token_rows = lax.all_to_all(gated, "tp", split_axis=0, concat_axis=1, tiled=True)
-    out_columns = lax.all_gather(w_mix_out, "fs", axis=1, tiled=True)
+    blocks = lax.all_gather(w_mix_out, "fs")
+    out_columns = jnp.concatenate(blocks, axis=1)
     out_whole = lax.all_gather(out_columns, "tp", axis=0, tiled=True)
     own_rows = lax.dynamic_slice_in_dim(tokens, row_start, half, 0)
     own_mid = (

time: 517 us -> 516 us (level)
  no operation moved by 1% of the time
where the time goes in v1:
time: 516 us
  waiting for transfers between devices  392 us (76%)
  matrix products  55.2 us (11%)
  other arithmetic  22.8 us (4%)
  local copies, waits for them, and re-layouts  18.2 us (4%)
  blocking collectives  13.7 us (3%)
  between operations  13.4 us (3%)
    all_gather x1, waiting for transfers between devices, on_device(): lax.all_gather(w_gate, 'fs', axis=0, tiled=True)  92.6 us
    all_gather x1, waiting for transfers between devices, on_device(): down_cols = lax.all_gather(w_down, 'fs', axis=1, tiled=True)  88.1 us
    all_gather x1, waiting for transfers between devices, on_device(): lax.all_gather(w_up, 'fs', axis=0, tiled=True)  80.8 us
    all_gather x1, waiting for transfers between devices, on_device(): blocks = lax.all_gather(w_mix_out, 'fs')  52.5 us
    all_gather x1, waiting for transfers between devices, on_device(): lax.all_gather(w_value, 'fs', axis=0, tiled=True)  41.9 us
    all_gather x1, waiting for transfers between devices, on_device(): lax.all_gather(w_unit, 'fs', axis=0, tiled=True)  15.5 us
    reduce_sum x1, other arithmetic, spatial_unit(): spread = jnp.mean(jnp.square(active - center), axis=-1, keepdims=True)  14.4 us
    all_gather x1, waiting for transfers between devices, on_device(): h_mid = lax.all_gather(own_mid, 'tp', axis=0, tiled=True)  13.2 us
  transfers between devices with their start and end apart: 9, of which 9 were waited for; matrix products, arithmetic and copies ran while one was open for 16% of the time, Pallas kernels for 0%

profile of v1, /device:TPU:0, one launch (start us, length us, event | category | flops | bytes accessed | tf_op | source)
XLA Modules:
  0.0 515.6 jit_solution(14128345839930899657)
XLA Ops:
  6.5 0.0 copy-start.2
  6.5 0.0 copy-start.6
  6.5 0.0 all-gather.27.cloned.1.call-start
  6.6 0.7 all-gather.27.cloned.1.call-update
  7.3 0.0 all-gather.13.cloned.1.call-start
  7.3 0.7 all-gather.13.cloned.1.call-update
  8.0 0.0 all-gather.11.cloned.1.call-start
  8.1 0.7 all-gather.11.cloned.1.call-update
  8.8 0.0 all-gather.15.cloned.1.call-start
  8.8 52.5 %all-gather.27.cloned.1.call-done = bf16[4096,256]{1,0:T(8,128)(2,1)} async-done(((bf16[512,256]{1,0:T(8,128)(2,1)}), bf16[4096,256]{1,0:T(8,128)(2,1)}) %all-gather.27.cloned.1.call-update) | async-done | bytes 2097168 | tf_op jit(solution)/shard_map/all_gather | solution.py:68
  61.3 3.9 copy.38
  65.3 0.0 all-gather.15.cloned.1.call-update
  65.3 0.0 all-gather.23.cloned.1.call-start
  65.3 0.5 all-gather.23.cloned.1.call-update
  65.9 0.0 all-gather.17.cloned.1.call-start
  65.9 0.0 copy-done.2
  66.0 0.0 copy-done.6
  66.0 0.0 copy-done.5
  66.0 0.0 copy-done.4
  66.0 0.1 dynamic-slice_convert_fusion
  66.1 3.1 fusion
  69.2 41.9 %all-gather.13.cloned.1.call-done = bf16[2048,512]{1,0:T(8,128)(2,1)} async-done(((bf16[256,512]{1,0:T(8,128)(2,1)}), bf16[2048,512]{1,0:T(8,128)(2,1)}) %all-gather.13.cloned.1.call-update) | async-done | bytes 2097168 | tf_op jit(solution)/shard_map/all_gather | solution.py:60
  111.1 6.9 %fusion.21 = f32[1024,512]{1,0:T(8,128)} fusion(bf16[2048,512]{1,0:T(8,128)(2,1)} %all-gather.13.cloned.1.call-done, bf16[1024,2048]{1,0:T(8,128)(2,1)} %param.13, f32[2048]{0:T(1024)S(1)} %convert_element_type.48, f32[1024]{0:T(1024)S(1)} %add_rsqrt_fusion.2), kind=kOutput, calls=%fused_computation.30 | convolution fusion | flops 2160066560 | bytes 8400896 | tf_op jit(solution)/shard_map/dot_general | solution.py:63
  118.0 2.6 reshape.64
  120.6 1.2 reduce_sum.37
  121.8 14.4 %multiply_reduce_fusion = f32[1024,2]{1,0:T(8,128)S(1)} fusion(f32[1024,2,256]{2,1,0:T(2,128)S(1)} %reshape.64, f32[1024,2]{1,0:T(8,128)S(1)} %broadcast_multiply_fusion), kind=kLoop, calls=%fused_computation.33 | loop fusion | flops 1570816 | bytes 2113536 | tf_op jit(solution)/shard_map/reduce_sum | solution.py:19
  136.3 0.1 add_rsqrt_fusion
  136.3 1.2 mul.113
  137.6 0.2 copy.43
  137.8 0.0 copy-start
  137.8 1.2 sub.17
  139.0 0.2 copy.42
  139.2 0.4 copy-done
  139.6 0.8 add_convert_fusion.2
  140.4 0.3 reshape.65
  140.7 0.0 copy-done.1
  140.7 0.5 bitcast_add_fusion
  141.3 2.3 copy.36
  143.6 1.8 copy.44
  145.4 15.5 %all-gather.11.cloned.1.call-done = bf16[2048,512]{1,0:T(8,128)(2,1)} async-done(((bf16[256,512]{1,0:T(8,128)(2,1)}), bf16[2048,512]{1,0:T(8,128)(2,1)}) %all-gather.11.cloned.1.call-update) | async-done | bytes 2097168 | tf_op jit(solution)/shard_map/all_gather | solution.py:59
  160.9 5.7 %fusion.14 = bf16[1024,512]{1,0:T(8,128)(2,1)S(1)} fusion(f32[1024,512]{1,0:T(8,128)S(1)} %bitcast.45, bf16[2048,512]{1,0:T(8,128)(2,1)} %all-gather.11.cloned.1.call-done, bf16[1024,2048]{1,0:T(8,128)(2,1)} %param.13, f32[2048]{0:T(1024)S(1)} %convert_element_type.48, f32[1024]{0:T(1024)S(1)} %add_rsqrt_fusion.2), kind=kOutput, calls=%fused_computation.23 | convolution fusion | flops 2161115136 | bytes 9449472 | tf_op jit(solution)/shard_map/dot_general | solution.py:62
  166.6 0.5 copy.37
  167.1 4.6 all_to_all.38
  171.7 2.8 all-gather.15.cloned.1.call-done
  174.5 6.6 %add_convert_fusion.1 = bf16[512,2048]{1,0:T(8,128)(2,1)} fusion(bf16[512,1024]{0,1:T(8,128)(2,1)S(1)} %bitcast.46, bf16[1024,2048]{0,1:T(8,128)(2,1)} %all-gather.15.cloned.1.call-done, bf16[1024,2048]{1,0:T(8,128)(2,1)} %param.13, s32[]{:T(128)S(6)} %select_n.16), kind=kOutput, calls=%fused_computation.12 | convolution fusion | flops 2150629376 | bytes 9437188 | tf_op jit(solution)/shard_map/dot_general | solution.py:74
  181.1 0.0 all-gather.17.cloned.1.call-update
  181.1 0.0 all-gather.19.cloned.1.call-start
  181.2 0.7 all-gather.19.cloned.1.call-update
  181.9 0.0 all-gather.21.cloned.1.call-start
  181.9 0.7 all-gather.21.cloned.1.call-update
  182.6 0.0 all-gather.25.cloned.1.call-start
  182.7 88.1 %all-gather.23.cloned.1.call-done = bf16[1408,2048]{1,0:T(8,128)(2,1)} async-done(((bf16[1408,256]{1,0:T(8,128)(2,1)}), bf16[1408,2048]{1,0:T(8,128)(2,1)}) %all-gather.23.cloned.1.call-update) | async-done | bytes 5767184 | tf_op jit(solution)/shard_map/all_gather | solution.py:85
  270.7 0.0 all-gather.25.cloned.1.call-update
  270.8 0.0 copy-done.3
  270.8 13.2 %all-gather.17.cloned.1.call-done = bf16[1024,2048]{1,0:T(8,128)(2,1)} async-done(((bf16[512,2048]{1,0:T(8,128)(2,1)}), bf16[1024,2048]{1,0:T(8,128)(2,1)}) %all-gather.17.cloned.1.call-update) | async-done | bytes 4194320 | tf_op jit(solution)/shard_map/all_gather | solution.py:76
  284.0 3.1 fusion.3
  287.1 92.6 %all-gather.19.cloned.1.call-done = bf16[2048,1408]{1,0:T(8,128)(2,1)} async-done(((bf16[256,1408]{1,0:T(8,128)(2,1)}), bf16[2048,1408]{1,0:T(8,128)(2,1)}) %all-gather.19.cloned.1.call-update) | async-done | bytes 5767184 | tf_op jit(solution)/shard_map/all_gather | solution.py:79
  379.7 11.9 %fusion.23 = f32[1024,1408]{1,0:T(8,128)} fusion(bf16[2048,1408]{1,0:T(8,128)(2,1)} %all-gather.19.cloned.1.call-done, bf16[1024,2048]{1,0:T(8,128)(2,1)} %all-gather.17.cloned.1.call-done, f32[2048]{0:T(1024)S(1)} %convert_element_type.57, f32[1024]{0:T(1024)S(1)} %add_rsqrt_fusion.1), kind=kOutput, calls=%fused_computation.34 | convolution fusion | flops 5913968640 | bytes 15740928 | tf_op jit(solution)/shard_map/dot_general | solution.py:82
  391.6 80.8 %all-gather.21.cloned.1.call-done = bf16[2048,1408]{1,0:T(8,128)(2,1)} async-done(((bf16[256,1408]{1,0:T(8,128)(2,1)}), bf16[2048,1408]{1,0:T(8,128)(2,1)}) %all-gather.21.cloned.1.call-update) | async-done | bytes 5767184 | tf_op jit(solution)/shard_map/all_gather | solution.py:80
  472.4 12.5 %multiply_convert_fusion = bf16[1024,1408]{1,0:T(8,128)(2,1)} fusion(f32[1024,1408]{1,0:T(8,128)} %fusion.23, bf16[2048,1408]{1,0:T(8,128)(2,1)} %all-gather.21.cloned.1.call-done, bf16[1024,2048]{1,0:T(8,128)(2,1)} %all-gather.17.cloned.1.call-done, f32[2048]{0:T(1024)S(1)} %convert_element_type.57, f32[1024]{0:T(1024)S(1)} %add_rsqrt_fusion.1), kind=kOutput, calls=%fused_computation.10 | convolution fusion | flops 5922619392 | bytes 18624512 | tf_op jit(solution)/shard_map/dot_general | solution.py:83
  484.9 3.4 copy.39
  488.4 9.1 %all_to_all.39 = bf16[2,512,1408]{1,2,0:T(8,128)(2,1)} all-to-all(bf16[2,512,1408]{1,2,0:T(8,128)(2,1)S(1)} %copy.39), channel_id=1, replica_groups=mesh['rep'=2,'fs'=8,'tp'=2] {'tp'}, dimensions={0} | all-to-all | bytes 5767168 | tf_op jit(solution)/shard_map/all_to_all | solution.py:87
  497.4 0.5 all-gather.25.cloned.1.call-done
  497.9 11.1 %add_convert_fusion = bf16[512,2048]{1,0:T(8,128)(2,1)} fusion(bf16[512,2816]{0,1:T(8,128)(2,1)} %bitcast.42, bf16[2816,2048]{1,0:T(8,128)(2,1)} %all-gather.25.cloned.1.call-done, bf16[1024,2048]{1,0:T(8,128)(2,1)} %all-gather.17.cloned.1.call-done, s32[]{:T(128)S(6)} %select_n.16), kind=kOutput, calls=%fused_computation.11 | convolution fusion | flops 5908725760 | bytes 18612228 | tf_op jit(solution)/shard_map/dot_general | solution.py:89
  (11 shorter events, 0.1 us)
Async XLA Ops:
  6.5 59.4 %copy-start.2 = (bf16[2048]{0:T(1024)(128)(2,1)S(1)}, bf16[2048]{0:T(1024)(128)(2,1)}, u32[]{:S(2)}) copy-start(bf16[2048]{0:T(1024)(128)(2,1)} %param.14) | copy-start | bytes 12292
  6.5 59.4 %copy-start.6 = (bf16[4,128]{1,0:T(4,128)(2,1)S(1)}, bf16[4,128]{1,0:T(4,128)(2,1)}, u32[]{:S(2)}) copy-start(bf16[4,128]{1,0:T(4,128)(2,1)} %param.18) | copy-start | bytes 3076
  6.5 59.4 %copy-start.5 = (bf16[1024]{0:T(1024)(128)(2,1)S(1)}, bf16[1024]{0:T(1024)(128)(2,1)}, u32[]{:S(2)}) copy-start(bf16[1024]{0:T(1024)(128)(2,1)} %param.19) | copy-start | bytes 6148
  6.5 59.5 %copy-start.4 = (bf16[1024]{0:T(1024)(128)(2,1)S(1)}, bf16[1024]{0:T(1024)(128)(2,1)}, u32[]{:S(2)}) copy-start(bf16[1024]{0:T(1024)(128)(2,1)} %param.20) | copy-start | bytes 6148
  6.5 54.8 %all-gather.27.cloned.1.call-start = ((), (), s32[]{:S(2)}) async-start(), calls=%async_computation.10 | async-start | bytes 2359296 | tf_op jit(solution)/shard_map/all_gather | solution.py:68
  7.3 103.8 %all-gather.13.cloned.1.call-start = ((), (), s32[]{:S(2)}) async-start(), calls=%async_computation.3 | async-start | bytes 2359296 | tf_op jit(solution)/shard_map/all_gather | solution.py:60
  8.0 152.9 %all-gather.11.cloned.1.call-start = ((), (), s32[]{:S(2)}) async-start(), calls=%async_computation.2 | async-start | bytes 2359296 | tf_op jit(solution)/shard_map/all_gather | solution.py:59
  8.8 165.8 %all-gather.15.cloned.1.call-start = ((), (), s32[]{:S(2)}) async-start(), calls=%async_computation.4 | async-start | bytes 6291456 | tf_op jit(solution)/shard_map/all_gather | solution.py:70
  65.3 205.5 %all-gather.23.cloned.1.call-start = ((), (), s32[]{:S(2)}) async-start(), calls=%async_computation.8 | async-start | bytes 6488064 | tf_op jit(solution)/shard_map/all_gather | solution.py:85
  65.9 218.1 %all-gather.17.cloned.1.call-start = ((), (), s32[]{:S(2)}) async-start(), calls=%async_computation.5 | async-start | bytes 6291456 | tf_op jit(solution)/shard_map/all_gather | solution.py:76
  137.8 1.9 copy-start
  139.6 1.1 copy-start.1
  181.1 89.7 %copy-start.3 = (bf16[2048]{0:T(1024)(128)(2,1)S(1)}, bf16[2048]{0:T(1024)(128)(2,1)}, u32[]{:S(2)}) copy-start(bf16[2048]{0:T(1024)(128)(2,1)} %param.22) | copy-start | bytes 12292
  181.1 198.6 %all-gather.19.cloned.1.call-start = ((), (), s32[]{:S(2)}) async-start(), calls=%async_computation.6 | async-start | bytes 6488064 | tf_op jit(solution)/shard_map/all_gather | solution.py:79
  181.9 290.6 %all-gather.21.cloned.1.call-start = ((), (), s32[]{:S(2)}) async-start(), calls=%async_computation.7 | async-start | bytes 6488064 | tf_op jit(solution)/shard_map/all_gather | solution.py:80
  182.6 315.3 %all-gather.25.cloned.1.call-start = ((), (), s32[]{:S(2)}) async-start(), calls=%async_computation.9 | async-start | bytes 17301504 | tf_op jit(solution)/shard_map/all_gather | solution.py:88
Sparse Core Ops, SparseCore 0:
  9.5 51.7 all-gather.26
  63.4 47.6 all-gather.12
  113.2 47.6 all-gather.10
  162.3 12.1 all-gather.14
  176.4 94.2 all-gather.22
  272.1 11.8 all-gather.16
  286.2 93.4 all-gather.18
  381.9 90.4 all-gather.20
  474.0 23.8 all-gather.24
